TPU v7x, 32 devices: a whole 2x2x4 slice. The times are simulated.
32 devices in a mesh: fs: 8 (over z, y), tp: 4 (over x, core).
Axes of the slice: x: 2, y: 2, z: 4, core: 2. Of those that a mesh axis runs over, the one named last changes fastest.
Arguments:
- prompt: bfloat16 [6144, 2048], P('fs'), may hold values from -6 to 6
- routes: int32 [6144, 2], P('fs'), may hold values from 0 to 15, all different within a row; in each aligned block of 768 rows (0 to 767, 768 to 1535, ...) at most 192 rows name the same one
- affinity: float32 [6144, 2], P('fs'), may hold values from 0.05 to 1
- norm_gain: float32 [2048], P('fs'), may hold values from 0.1 to 1.9
- gate_master: float32 [16, 2048, 1024], P(None, 'fs', 'tp'), may hold values from -0.125 to 0.125
- up_master: float32 [16, 2048, 1024], P(None, 'fs', 'tp'), may hold values from -0.125 to 0.125
- down_master: float32 [16, 1024, 2048], P(None, 'fs', 'tp'), may hold values from -0.1875 to 0.1875
Outputs:
- mixed: bfloat16 [6144, 2048], P('fs', 'tp')
- gate_weights: bfloat16 [16, 2048, 1024], P('fs', None, 'tp')
- up_weights: bfloat16 [16, 2048, 1024], P('fs', None, 'tp')
- down_weights: bfloat16 [16, 1024, 2048], P('fs', None, 'tp')
Inputs may be any that keep to these rules, and one draw needn't show every extreme that they name: `routes`: each row names 2 different experts. In each aligned block of 768 rows no expert is named more than 192 times, a bound that some block reaches.
All inputs are finite; a program needn't handle non-finite values.
Results may differ from a plain program's by a relative error of at most 0.0086.
Values may be sent and summed in bfloat16 or wider, within the bound.
A program may use at most 128 MiB of HBM per device.

v0:
```python
import functools

import jax
import jax.numpy as jnp
from jax import lax
from jax.experimental import pallas as pl
from jax.experimental.pallas import tpu as pltpu
from jax.sharding import PartitionSpec as P

norm_eps = 1e-06
MESH = pl.DeviceIdType.MESH


def remote(src, dst, send_sem, recv_sem, where):
    return pltpu.make_async_remote_copy(
        src_ref=src,
        dst_ref=dst,
        send_sem=send_sem,
        recv_sem=recv_sem,
        device_id=where,
        device_id_type=MESH,
    )


def loop(first, last, body):
    def step(i, carry):
        body(i)
        return carry

    lax.fori_loop(first, last, step, 0)


class Spread:
    def __init__(self, tp, whole, rows_of, width, sems):
        self.chips = tp // 2
        self.me = lax.axis_index("tp")
        self.chip, self.core = self.me // 2, self.me % 2
        self.whole, self.rows_of, self.width = whole, rows_of, width
        self.first_send, self.first_recv, self.relay_send, self.relay_recv = sems

    def greet(self, barrier):
        for hop in range(self.chips):
            pl.semaphore_signal(barrier, inc=1, device_id={"tp": self.target(hop)}, device_id_type=MESH)
        return self.chips

    def target(self, hop):
        if hop == 0:
            return self.chip * 2 + 1 - self.core
        return lax.rem(self.chip + hop, self.chips) * 2 + self.core

    def block(self, chunk, owner):
        return self.whole.at[:, self.rows_of(chunk), pl.ds(pl.multiple_of(owner * self.width, self.width), self.width)]

    def first(self, chunk, hop):
        mine = self.block(chunk, self.me)
        return remote(mine, mine, self.first_send.at[chunk, hop], self.first_recv.at[chunk, hop], {"tp": self.target(hop)})

    def relay(self, chunk, hop):
        owner = lax.rem(self.chip - hop + self.chips, self.chips) * 2 + self.core
        taken = self.block(chunk, owner)
        return remote(taken, taken, self.relay_send.at[chunk, hop], self.relay_recv.at[chunk, hop], {"tp": self.target(0)})

    def start(self, chunk):
        for hop in [*range(1, self.chips), 0]:
            self.first(chunk, hop).start()

    def hand_on(self, chunk):
        for hop in range(1, self.chips):
            self.first(chunk, hop).wait_recv()
            self.relay(chunk, hop).start()

    def finish(self, chunk):
        self.first(chunk, 0).wait_recv()
        for hop in range(self.chips):
            self.first(chunk, hop).wait_send()
        for hop in range(1, self.chips):
            self.relay(chunk, hop).wait()


def spread_sems(n, tp):
    return [pltpu.SemaphoreType.DMA((n, tp // 2))] * 4


def peer(step, n):
    return lax.rem(lax.axis_index("fs") + step, n)


def source(step, n):
    return lax.rem(lax.axis_index("fs") - step + n, n)


class Weights:
    def __init__(self, n, master, gain, out, raw, send, sems):
        self.n, self.master, self.gain, self.out, self.raw, self.send = n, master, gain, out, raw, send
        self.load_sem, self.send_sem, self.recv_sem = sems
        self.keep, self.rows = master.shape[0] // n, master.shape[1]

    def load(self, step):
        return pltpu.make_async_copy(
            self.master.at[pl.ds(peer(step, self.n) * self.keep, self.keep)], self.raw.at[step], self.load_sem.at[step]
        )

    def place(self):
        me = lax.axis_index("fs")
        return self.out.at[:, pl.ds(pl.multiple_of(me * self.rows, self.rows), self.rows), :]

    def copy(self, step):
        return remote(
            self.send.at[step], self.place(), self.send_sem.at[step], self.recv_sem.at[step], {"fs": peer(step, self.n)}
        )

    def own(self):
        return pltpu.make_async_copy(self.send.at[0], self.place(), self.send_sem.at[0])

    def load_all(self):
        for step in [*range(1, self.n), 0]:
            self.load(step).start()

    def cast(self, step):
        self.load(step).wait()
        block = self.raw[step]
        if self.gain is not None:
            block = block * self.gain[...][None]
        self.send[step] = block.astype(jnp.bfloat16)

    def send_all(self):
        self.cast(1)

        def body(step):
            self.cast(step)
            self.copy(step - 1).start()

        loop(2, self.n, body)
        self.cast(0)
        self.copy(self.n - 1).start()
        self.own().start()

    def finish(self):
        self.own().wait()
        loop(1, self.n, lambda step: self.copy(step).wait())


def greet_all(n, spread):
    barrier = pltpu.get_barrier_semaphore()
    for step in range(1, n):
        pl.semaphore_signal(barrier, inc=1, device_id={"fs": peer(step, n)}, device_id_type=MESH)
    amount = spread.greet(barrier)
    pl.semaphore_wait(barrier, n - 1 + amount)


def dispatch_kernel(n, tp, gain, outbox, gate, up, gate_out, up_out, gathered, *refs):
    gate_raw, up_raw, gate_send, up_send, weight_sems, token_send, token_recv = refs[:7]
    keep, (_, capacity, width) = outbox.shape[0] // n, outbox.shape
    me = lax.axis_index("fs")
    parts = [
        Weights(n, gate, gain, gate_out, gate_raw, gate_send, [weight_sems.at[0, i] for i in range(3)]),
        Weights(n, up, gain, up_out, up_raw, up_send, [weight_sems.at[1, i] for i in range(3)]),
    ]

    def rows_of(chunk):
        return pl.ds(pl.multiple_of(source(chunk, n) * capacity, capacity), capacity)

    spread = Spread(tp, gathered, rows_of, width, refs[7:11])
    column = pl.ds(pl.multiple_of(lax.axis_index("tp") * width, width), width)

    def token(step):
        return remote(
            outbox.at[pl.ds(peer(step, n) * keep, keep)],
            gathered.at[:, pl.ds(pl.multiple_of(me * capacity, capacity), capacity), column],
            token_send.at[step],
            token_recv.at[step],
            {"fs": peer(step, n)},
        )

    own = pltpu.make_async_copy(
        outbox.at[pl.ds(me * keep, keep)], spread.block(0, lax.axis_index("tp")), token_send.at[0]
    )
    own.start()
    for part in parts:
        part.load_all()
    greet_all(n, spread)
    loop(1, n, lambda step: token(step).start())
    own.wait()
    spread.start(0)
    for part in parts:
        part.send_all()

    def body(step):
        token(step).wait_recv()
        spread.start(step)
        spread.hand_on(step - 1)

    loop(1, n, body)
    spread.hand_on(n - 1)
    loop(1, n, lambda step: token(step).wait_send())
    loop(0, n, spread.finish)
    for part in parts:
        part.finish()


def weight_shapes(master, n):
    experts, rows, columns = master.shape
    keep = experts // n
    return (
        jax.ShapeDtypeStruct((keep, rows * n, columns), jnp.bfloat16),
        pltpu.VMEM((n, keep, rows, columns), jnp.float32),
        pltpu.VMEM((n, keep, rows, columns), jnp.bfloat16),
    )


def dispatch(gain, outbox, gate, up):
    n, tp = lax.axis_size("fs"), lax.axis_size("tp")
    experts, capacity, width = outbox.shape
    gate_out, gate_raw, gate_send = weight_shapes(gate, n)
    up_out, up_raw, up_send = weight_shapes(up, n)
    inside, anywhere = pl.BlockSpec(memory_space=pltpu.VMEM), pl.BlockSpec(memory_space=pl.ANY)
    return pl.pallas_call(
        functools.partial(dispatch_kernel, n, tp),
        out_shape=[
            gate_out,
            up_out,
            jax.ShapeDtypeStruct((experts // n, n * capacity, width * tp), jnp.bfloat16),
        ],
        in_specs=[inside, inside, anywhere, anywhere],
        out_specs=[anywhere] * 3,
        scratch_shapes=[gate_raw, up_raw, gate_send, up_send]
        + [pltpu.SemaphoreType.DMA((2, 3, n))]
        + [pltpu.SemaphoreType.DMA((n,))] * 2
        + spread_sems(n, tp),
        compiler_params=pltpu.CompilerParams(
            collective_id=0, has_side_effects=True, vmem_limit_bytes=48 * 2**20
        ),
        name="dispatch",
    )(gain[:, None], outbox, gate, up)


def combine_kernel(n, tp, gathered, gate, up, down, down_out, returned, *refs):
    raw, send, held, whole, out, taken, gate_in, up_in = refs[:8]
    weight_sems, back_send, back_recv, local_sem, in_sem = refs[8:13]
    keep, rows, _ = gathered.shape
    width = gate.shape[2]
    capacity = rows // n
    me = lax.axis_index("fs")
    part = Weights(n, down, None, held, raw, send, [weight_sems.at[i] for i in range(3)])

    def rows_of(chunk):
        return pl.ds(pl.multiple_of(peer(chunk, n) * capacity, capacity), capacity)

    spread = Spread(tp, whole, rows_of, width, refs[13:17])
    column = pl.ds(pl.multiple_of(lax.axis_index("tp") * width, width), width)

    def take(chunk):
        return pltpu.make_async_copy(
            gathered.at[:, rows_of(chunk), :], taken.at[:, rows_of(chunk), :], in_sem.at[chunk]
        )

    weights = [
        pltpu.make_async_copy(gate, gate_in, in_sem.at[n]),
        pltpu.make_async_copy(up, up_in, in_sem.at[n + 1]),
    ]

    part.load_all()
    for weight in weights:
        weight.start()
    loop(0, n, lambda chunk: take(chunk).start())
    greet_all(n, spread)
    part.send_all()
    for weight in weights:
        weight.wait()

    def produce(chunk):
        take(chunk).wait()
        for e in range(keep):
            block = taken[e, rows_of(chunk), :]
            gate_pre = jnp.dot(block, gate_in[e], preferred_element_type=jnp.float32)
            up_pre = jnp.dot(block, up_in[e], preferred_element_type=jnp.float32)
            hidden = gate_pre / (1.0 + jnp.exp(-gate_pre)) * up_pre
            whole[e, rows_of(chunk), column] = hidden.astype(jnp.bfloat16)

    def advance(chunk):
        produce(chunk)
        spread.start(chunk - 1)
        spread.hand_on(chunk - 2)

    produce(0)
    produce(1)
    spread.start(0)
    loop(2, n, advance)
    spread.start(n - 1)
    loop(n - 2, n, spread.hand_on)
    loop(0, n, spread.finish)
    part.finish()
    keeping = pltpu.make_async_copy(held, down_out, local_sem.at[0])
    keeping.start()

    def back(step):
        return remote(
            out.at[step], returned.at[me], back_send.at[step], back_recv.at[step], {"fs": peer(step, n)}
        )

    def multiply(step):
        for e in range(keep):
            out[step, e] = jnp.dot(
                whole[e, rows_of(step), :], held[e], preferred_element_type=jnp.float32
            ).astype(jnp.bfloat16)

    multiply(1)

    def body(step):
        multiply(step)
        back(step - 1).start()

    loop(2, n, body)
    multiply(0)
    back(n - 1).start()
    mine = pltpu.make_async_copy(out.at[0], returned.at[me], back_send.at[0])
    mine.start()
    keeping.wait()
    mine.wait()
    loop(1, n, lambda step: back(step).wait())


def combine(gathered, gate, up, down):
    n, tp = lax.axis_size("fs"), lax.axis_size("tp")
    (keep, rows, _), width = gathered.shape, gate.shape[2]
    down_out, raw, send = weight_shapes(down, n)
    columns = down.shape[2]
    block = (n, keep, rows // n, columns)
    anywhere = pl.BlockSpec(memory_space=pl.ANY)
    return pl.pallas_call(
        functools.partial(combine_kernel, n, tp),
        out_shape=[down_out, jax.ShapeDtypeStruct(block, jnp.bfloat16)],
        in_specs=[anywhere] * 4,
        out_specs=[anywhere] * 2,
        scratch_shapes=[
            raw,
            send,
            pltpu.VMEM(down_out.shape, jnp.bfloat16),
            pltpu.VMEM((keep, rows, width * tp), jnp.bfloat16),
            pltpu.VMEM(block, jnp.bfloat16),
            pltpu.VMEM(gathered.shape, jnp.bfloat16),
            pltpu.VMEM(gate.shape, jnp.bfloat16),
            pltpu.VMEM(up.shape, jnp.bfloat16),
            pltpu.SemaphoreType.DMA((3, n)),
            pltpu.SemaphoreType.DMA((n,)),
            pltpu.SemaphoreType.DMA((n,)),
            pltpu.SemaphoreType.DMA((n,)),
            pltpu.SemaphoreType.DMA((n + 2,)),
        ]
        + spread_sems(n, tp),
        compiler_params=pltpu.CompilerParams(
            collective_id=1, has_side_effects=True, vmem_limit_bytes=48 * 2**20
        ),
        name="combine",
    )(gathered, gate, up, down)


def per_device(prompt, routes, affinity, norm_gain, gate_master, up_master, down_master):
    tp_count = lax.axis_size("tp")
    experts = gate_master.shape[0]
    token_count, model_width = prompt.shape
    top_count = routes.shape[1]
    capacity = 2 * token_count * top_count // experts

    values = prompt.astype(jnp.float32)
    scale = lax.rsqrt(jnp.mean(values * values, axis=-1, keepdims=True) + norm_eps)
    column_width = model_width // tp_count
    columns = lax.dynamic_slice_in_dim(
        prompt, lax.axis_index("tp") * column_width, column_width, 1
    )
    normed = (columns.astype(jnp.float32) * scale).astype(jnp.bfloat16)

    names = jnp.arange(experts, dtype=jnp.int32)
    hits = (routes.T[:, None, :] == names[None, :, None]).astype(jnp.float32)
    named = jnp.sum(hits, axis=0)
    position = jnp.arange(token_count, dtype=jnp.int32)
    earlier = (position[:, None] < position[None, :]).astype(jnp.bfloat16)
    rank = jnp.dot(named.astype(jnp.bfloat16), earlier, preferred_element_type=jnp.float32)
    slot = jnp.where(named > 0, rank, -1.0).astype(jnp.int32)
    share = (affinity / jnp.sum(affinity, axis=1, keepdims=True)).T
    weight = jnp.sum(hits * share[:, None, :], axis=0)

    places = jnp.arange(capacity, dtype=jnp.int32)
    pick = (slot[:, None, :] == places[None, :, None]).astype(jnp.bfloat16)
    outbox = jnp.einsum(
        "ert,td->erd", pick, normed, preferred_element_type=jnp.float32
    ).astype(jnp.bfloat16)

    gate_new, up_new, gathered = dispatch(norm_gain, outbox, gate_master, up_master)
    down_new, returned = combine(gathered, gate_new, up_new, down_master)

    spread = jnp.where(
        slot[:, None, :] == places[None, :, None], weight[:, None, :], 0
    ).astype(jnp.bfloat16)
    mixed = lax.dot_general(
        spread.reshape(experts * capacity, token_count),
        returned.reshape(experts * capacity, -1),
        (((0,), (0,)), ((), ())),
        preferred_element_type=jnp.float32,
    ).astype(jnp.bfloat16)
    return (mixed, gate_new, up_new, down_new)


def solution(mesh):
    in_specs = (
        P("fs", None),
        P("fs", None),
        P("fs", None),
        P("fs"),
        P(None, "fs", "tp"),
        P(None, "fs", "tp"),
        P(None, "fs", "tp"),
    )
    out_specs = (P("fs", "tp"), P("fs", None, "tp"), P("fs", None, "tp"), P("fs", None, "tp"))
    return jax.shard_map(
        per_device, mesh=mesh, in_specs=in_specs, out_specs=out_specs, check_vma=False
    )
```

profile of v0, /device:TPU:28, one launch (start us, length us, event | category | flops | bytes accessed | tf_op | source)
XLA Modules:
  0.0 318.9 jit_solution(15345253532513571530)
XLA Ops:
  0.6 0.7 reduce_sum.37
  1.3 0.7 divide_bitcast_fusion
  2.0 0.7 convert_reduce_fusion
  2.8 0.2 fusion.5
  3.0 2.6 multiply_reduce_fusion
  5.6 0.0 copy-start.2
  5.6 5.3 %fusion.3.outbox = bf16[16,192,512]{2,1,0:T(8,128)(2,1)} fusion(s32[16,768]{1,0:T(8,128)S(1)} %fusion.5, f32[768]{0:T(1024)S(1)} %add_rsqrt_fusion, bf16[768,2048]{1,0:T(8,128)(2,1)} %param.7, s32[]{:T(128)S(6)} %select_n.21), kind=kOutput, calls=%fused_computation.7 | convolution fusion | flops 2421030912 | bytes 3984388 | tf_op jit(solution)/shard_map/ert,td->erd/dot_general | solution.py:385
  10.9 0.0 copy-done.2
  10.9 0.1 copy.12.gain
  11.0 164.7 %dispatch.1 = (bf16[2,2048,256]{2,1,0:T(8,128)(2,1)S(1)}, bf16[2,2048,256]{2,1,0:T(8,128)(2,1)S(1)}, bf16[2,1536,2048]{2,1,0:T(8,128)(2,1)}) custom-call(f32[256,1]{1,0:T(8,128)S(1)} %copy.12.gain, bf16[16,192,512]{2,1,0:T(8,128)(2,1)} %fusion.3.outbox, f32[16,256,256]{2,1,0:T(8,128)} %gate.1, f32[16,256,256]{2,1,0:T(8,128)} %up.1), custom_call_target="tpu_custom_call" | custom-call | tf_op jit(solution)/shard_map/dispatch/pallas_call | solution.py:217
  175.8 0.0 copy-start
  175.8 1.3 copy-done
  177.1 131.4 %combine.1 = (bf16[2,1024,512]{2,1,0:T(8,128)(2,1)S(1)}, bf16[8,2,192,512]{3,2,1,0:T(8,128)(2,1)}) custom-call(bf16[2,1536,2048]{2,1,0:T(8,128)(2,1)} %get-tuple-element.9.gathered, bf16[2,2048,256]{2,1,0:T(8,128)(2,1)S(1)} %get-tuple-element.21.gate, bf16[2,2048,256]{2,1,0:T(8,128)(2,1)} %copy-done, f32[16,128,512]{2,1,0:T(8,128)} %down.1), custom_call_target="tpu_custom_call" | custom-call | tf_op jit(solution)/shard_map/combine/pallas_call | solution.py:330
  308.5 0.0 copy-start.3
  308.5 1.7 select_convert_fusion
  310.3 0.1 copy-done.3
  310.4 3.5 %convolution_convert_fusion = bf16[768,512]{1,0:T(8,128)(2,1)} fusion(bf16[3072,768]{1,0:T(8,128)(2,1)S(1)} %bitcast.11, bf16[3072,512]{1,0:T(8,128)(2,1)S(1)} %bitcast.14), kind=kOutput, calls=%fused_computation.9 | convolution fusion | flops 2416312320 | bytes 8650752 | tf_op jit(solution)/shard_map/dot_general | solution.py:395
  313.9 0.0 copy-start.1
  313.9 1.3 copy.16
  315.2 1.0 copy-done.1
  316.3 1.3 copy.17
  317.6 1.3 copy.18
  (1 shorter events, 0.0 us)
Async XLA Ops:
  5.6 5.3 %copy-start.2 = (f32[256]{0:T(256)S(1)}, f32[256]{0:T(256)}, u32[]{:S(2)}) copy-start(f32[256]{0:T(256)} %param.10) | copy-start | bytes 3076
  175.8 1.3 copy-start
  308.5 1.9 copy-start.3
  313.9 2.3 copy-start.1
where the time goes:
time: 319 us
  Pallas kernels  296 us (93%)
  matrix products  9.02 us (3%)
  local copies, waits for them, and re-layouts  6.58 us (2%)
  other arithmetic  6.44 us (2%)
    pallas_call x1, Pallas kernels, dispatch(): pl.pallas_call(functools.partial(dispatch_kernel, n, tp), out_shape=[gate...  165 us
    pallas_call x1, Pallas kernels, combine(): pl.pallas_call(functools.partial(combine_kernel, n, tp), out_shape=[down_...  131 us
    unnamed x11, local copies, waits for them, and re-layouts  6.45 us

commit v1 on v0

v1 whole, which is shorter than its diff:
```python
import functools

import jax
import jax.numpy as jnp
from jax import lax
from jax.experimental import pallas as pl
from jax.experimental.pallas import tpu as pltpu
from jax.sharding import PartitionSpec as P

norm_eps = 1e-06
MESH = pl.DeviceIdType.MESH
RING = 4


def remote(src, dst, send_sem, recv_sem, where):
    return pltpu.make_async_remote_copy(
        src_ref=src,
        dst_ref=dst,
        send_sem=send_sem,
        recv_sem=recv_sem,
        device_id=where,
        device_id_type=MESH,
    )


def loop(first, last, body):
    def step(i, carry):
        body(i)
        return carry

    lax.fori_loop(first, last, step, 0)


def span(index, size):
    return pl.ds(pl.multiple_of(index * size, size), size)


def far_first(z, depth, i):
    low, high = z, depth - 1 - z
    skew = jnp.abs(low - high)
    reach = jnp.minimum(low, high)
    j = i - skew
    distance = reach - j // 2
    paired = jnp.where(j % 2 == 0, z + distance, z - distance)
    single = jnp.where(low > high, i, depth - 1 - i)
    return jnp.where(i < skew, single, paired)


class Spread:
    def __init__(self, tp, whole, rows, width, sems):
        self.chips = tp // 2
        self.me = lax.axis_index("tp")
        self.chip, self.core = self.me // 2, self.me % 2
        self.whole, self.rows, self.width = whole, rows, width
        self.first_send, self.first_recv, self.relay_send, self.relay_recv = sems

    def target(self, hop):
        if hop == 0:
            return self.chip * 2 + 1 - self.core
        return lax.rem(self.chip + hop, self.chips) * 2 + self.core

    def block(self, chunk, owner):
        return self.whole.at[:, span(chunk, self.rows), span(owner, self.width)]

    def first(self, chunk, hop):
        mine = self.block(chunk, self.me)
        return remote(mine, mine, self.first_send.at[chunk, hop], self.first_recv.at[chunk, hop], {"tp": self.target(hop)})

    def relay(self, chunk, hop):
        owner = lax.rem(self.chip - hop + self.chips, self.chips) * 2 + self.core
        taken = self.block(chunk, owner)
        return remote(taken, taken, self.relay_send.at[chunk, hop], self.relay_recv.at[chunk, hop], {"tp": self.target(0)})

    def start(self, chunk):
        for hop in [*range(1, self.chips), 0]:
            self.first(chunk, hop).start()

    def hand_on(self, chunk):
        for hop in range(1, self.chips):
            self.first(chunk, hop).wait_recv()
            self.relay(chunk, hop).start()

    def arrive(self, chunk):
        self.first(chunk, 0).wait_recv()
        for hop in range(1, self.chips):
            self.relay(chunk, hop).wait_recv()

    def drain(self, chunk):
        for hop in range(self.chips):
            self.first(chunk, hop).wait_send()
        for hop in range(1, self.chips):
            self.relay(chunk, hop).wait_send()


def spread_sems(chunks, tp):
    return [pltpu.SemaphoreType.DMA((chunks, tp // 2))] * 4


class Weights:
    def __init__(self, n, master, gain, held, raw, send, load_sem, send_sem, recv_sem):
        self.n, self.master, self.gain, self.held, self.raw, self.send = n, master, gain, held, raw, send
        self.load_sem, self.send_sem, self.recv_sem = load_sem, send_sem, recv_sem
        self.keep, self.rows = master.shape[0] // n, master.shape[1]
        self.me = lax.axis_index("fs")

    def load(self, turn, peer):
        slot = lax.rem(turn, RING)
        return pltpu.make_async_copy(
            self.master.at[pl.ds(peer * self.keep, self.keep)], self.raw.at[slot], self.load_sem.at[slot]
        )

    def taken(self, turn):
        block = self.raw[lax.rem(turn, RING)]
        if self.gain is not None:
            block = block * self.gain[...][None]
        return block.astype(jnp.bfloat16)

    def cast(self, turn):
        self.send[turn] = self.taken(turn)

    def place(self, source):
        return self.held.at[:, span(source, self.rows), :]

    def keep_own(self, turn):
        self.held[:, span(self.me, self.rows), :] = self.taken(turn)

    def copy(self, turn, peer):
        return remote(
            self.send.at[turn], self.place(self.me), self.send_sem.at[peer], self.recv_sem.at[self.me], {"fs": peer}
        )

    def arrival(self, source):
        return remote(
            self.send.at[0], self.place(source), self.send_sem.at[source], self.recv_sem.at[source], {"fs": source}
        )


def kernel(
    n,
    tp,
    deep,
    gain,
    routes,
    affinity,
    prompt,
    gate,
    up,
    down,
    mixed_out,
    gate_out,
    up_out,
    down_out,
    raw_gate,
    raw_up,
    raw_down,
    send_gate,
    send_up,
    send_down,
    held_pair,
    held_down,
    prompt_in,
    token,
    info,
    gathered,
    passed,
    hidden,
    results,
    arrived,
    mixed,
    spread_weight,
    total,
    load_sem,
    weight_send,
    weight_recv,
    prompt_sem,
    token_send,
    token_recv,
    info_send,
    info_recv,
    pass_send,
    pass_recv,
    result_send,
    result_recv,
    part_send,
    part_recv,
    out_sem,
    *spreads,
):
    wide = n // deep
    keep, capacity = passed.shape[2], passed.shape[3]
    tokens, width = token.shape[1], token.shape[2]
    units = gate.shape[2]
    experts = keep * n
    me = lax.axis_index("fs")
    z, y = me // wide, lax.rem(me, wide)
    column = span(lax.axis_index("tp"), width)

    rows_spread = Spread(tp, gathered, capacity, width, spreads[:4])
    unit_spread = Spread(tp, hidden, wide * capacity, units, spreads[4:])
    pair = [
        Weights(
            n, master, gain, held_pair.at[:, :, i * units : (i + 1) * units], raw, send,
            load_sem.at[i], weight_send.at[i], weight_recv.at[i],
        )
        for i, (master, raw, send) in enumerate([(gate, raw_gate, send_gate), (up, raw_up, send_up)])
    ]
    lower = Weights(n, down, None, held_down, raw_down, send_down, load_sem.at[2], weight_send.at[2], weight_recv.at[2])

    def place(i):
        return far_first(z, deep, i)

    def peer(turn):
        return place(turn // wide) * wide + lax.rem(y + 1 + lax.rem(turn, wide), wide)

    barrier = pltpu.get_barrier_semaphore()
    for step in range(1, n):
        pl.semaphore_signal(barrier, inc=1, device_id={"fs": lax.rem(me + step, n)}, device_id_type=MESH)
    for hop in range(rows_spread.chips):
        pl.semaphore_signal(barrier, inc=1, device_id={"tp": rows_spread.target(hop)}, device_id_type=MESH)
    fetch = pltpu.make_async_copy(prompt, prompt_in, prompt_sem.at[0])
    fetch.start()
    for part in [*pair, lower]:
        for turn in range(RING):
            part.load(turn, peer(turn)).start()

    r0, r1 = routes[0:1, :], routes[1:2, :]
    names = lax.broadcasted_iota(jnp.int32, (experts, tokens), 0)
    hit0 = (names == r0).astype(jnp.float32)
    hit1 = (names == r1).astype(jnp.float32)
    before = lax.broadcasted_iota(jnp.int32, (tokens, tokens), 0)
    after = lax.broadcasted_iota(jnp.int32, (tokens, tokens), 1)
    earlier = jnp.where(before < after, 1.0, 0.0).astype(jnp.bfloat16)
    rank = jnp.dot((hit0 + hit1).astype(jnp.bfloat16), earlier, preferred_element_type=jnp.float32)
    a0, a1 = affinity[0:1, :], affinity[1:2, :]
    whole = a0 + a1
    info[z] = jnp.concatenate(
        [
            r0.astype(jnp.float32),
            r1.astype(jnp.float32),
            jnp.sum(hit0 * rank, axis=0, keepdims=True),
            jnp.sum(hit1 * rank, axis=0, keepdims=True),
            a0 / whole,
            a1 / whole,
            a0,
            a1,
        ],
        axis=0,
    )
    fetch.wait()
    tile = 128

    def normalize(i):
        rows = span(i, tile)
        values = prompt_in[rows, :].astype(jnp.float32)
        scale = lax.rsqrt(jnp.mean(values * values, axis=-1, keepdims=True) + norm_eps)
        token[z, rows, :] = (prompt_in[rows, column].astype(jnp.float32) * scale).astype(jnp.bfloat16)

    loop(0, tokens // tile, normalize)
    pl.semaphore_wait(barrier, n - 1 + rows_spread.chips)

    def onward(zs, side):
        where = {"fs": me + side * wide}
        return [
            remote(token.at[zs], token.at[zs], token_send.at[zs, (side + 1) // 2], token_recv.at[zs], where),
            remote(info.at[zs], info.at[zs], info_send.at[zs, (side + 1) // 2], info_recv.at[zs], where),
        ]

    def sends(zs, act):
        @pl.when((zs <= z) & (z < deep - 1))
        def _():
            for copy in onward(zs, 1):
                act(copy)

        @pl.when((zs >= z) & (z > 0))
        def _():
            for copy in onward(zs, -1):
                act(copy)

    def entry_slot(zs, expert):
        facts = info[zs]
        name = expert.astype(jnp.float32)
        first, second = facts[0:1, :] == name, facts[1:2, :] == name
        slot = jnp.where(first, facts[2:3, :], jnp.where(second, facts[3:4, :], -1.0))
        weight = jnp.where(first, facts[4:5, :], facts[5:6, :])
        return slot, weight

    slots = lax.broadcasted_iota(jnp.int32, (capacity, tokens), 0).astype(jnp.float32)

    def pick(zs, row, e):
        slot, _ = entry_slot(zs, (z * wide + row) * keep + e)
        chosen = jnp.where(slots == slot, 1.0, 0.0).astype(jnp.bfloat16)
        return jnp.dot(chosen, token[zs], preferred_element_type=jnp.float32).astype(jnp.bfloat16)

    def passing(zs, row):
        return remote(
            passed.at[zs, row],
            gathered.at[:, span(zs * wide + y, capacity), column],
            pass_send.at[zs, row],
            pass_recv.at[zs * wide + y],
            {"fs": z * wide + row},
        )

    def passing_in(zs, row):
        return remote(
            passed.at[zs, row],
            gathered.at[:, span(zs * wide + row, capacity), column],
            pass_send.at[zs, row],
            pass_recv.at[zs * wide + row],
            {"fs": z * wide + row},
        )

    def others(act):
        for step in range(1, wide):
            act(lax.rem(y + step, wide))

    def near_first(i):
        return place(deep - 1 - i)

    def extract(zs):
        def give(row):
            for e in range(keep):
                passed[zs, row, e] = pick(zs, row, e)
            passing(zs, row).start()

        others(give)
        for e in range(keep):
            gathered[e, span(zs * wide + y, capacity), column] = pick(zs, y, e)
        rows_spread.start(zs * wide + y)

    def take_passed(zs):
        def take(row):
            passing_in(zs, row).wait_recv()
            rows_spread.start(zs * wide + row)

        others(take)

    def hand_on_passed(zs):
        others(lambda row: rows_spread.hand_on(zs * wide + row))

    def give_weights(parts, first, last):
        def body(turn):
            target = peer(turn)
            for part in parts:
                part.load(turn, target).wait()
                part.cast(turn)

                @pl.when(turn + RING < n)
                def _():
                    part.load(turn + RING, peer(turn + RING)).start()

                part.copy(turn, target).start()

        loop(first, last, body)

    sends(z, lambda copy: copy.start())
    extract(z)

    def hop(i):
        zs = near_first(i)
        for copy in onward(zs, 0):
            copy.wait_recv()
        sends(zs, lambda copy: copy.start())
        extract(zs)
        before = near_first(i - 1)
        take_passed(before)
        rows_spread.hand_on(before * wide + y)

        @pl.when(i >= 2)
        def _():
            hand_on_passed(near_first(i - 2))

        first = jnp.where(i == 1, 0, (i - 1) * (n - 1) // deep)
        last = i * (n - 1) // deep
        give_weights(pair, first, last)

    loop(1, deep, hop)
    give_weights(pair, (deep - 1) * (n - 1) // deep, n - 1)
    final = near_first(deep - 1)
    take_passed(final)
    hand_on_passed(near_first(deep - 2))
    give_weights([lower], 0, n - 1)
    rows_spread.hand_on(final * wide + y)
    hand_on_passed(final)
    for part in [*pair, lower]:
        part.load(n - 1, me).wait()
        part.keep_own(n - 1)
    loop(0, n, rows_spread.arrive)

    def settle(zs):
        sends(zs, lambda copy: copy.wait_send())
        others(lambda row: passing(zs, row).wait_send())

    def all_in(parts):
        def body(step):
            source = lax.rem(me + step, n)
            for part in parts:
                part.arrival(source).wait_recv()

        loop(1, n, body)

    all_in(pair)
    keeping = [
        pltpu.make_async_copy(held_pair.at[:, :, :units], gate_out, out_sem.at[0]),
        pltpu.make_async_copy(held_pair.at[:, :, units:], up_out, out_sem.at[1]),
        pltpu.make_async_copy(held_down, down_out, out_sem.at[2]),
    ]
    keeping[0].start()
    keeping[1].start()
    unit_column = span(lax.axis_index("tp"), units)
    group = wide * capacity

    def produce(i):
        zs = place(i)
        for e in range(keep):
            both = jnp.dot(gathered[e, span(zs, group), :], held_pair[e], preferred_element_type=jnp.float32)
            gate_pre, up_pre = both[:, :units], both[:, units:]
            hidden[e, span(zs, group), unit_column] = (
                gate_pre / (1.0 + jnp.exp(-gate_pre)) * up_pre
            ).astype(jnp.bfloat16)
        unit_spread.start(zs)

    produce(0)

    def advance(i):
        produce(i)
        unit_spread.hand_on(place(i - 1))

    loop(1, deep, advance)
    unit_spread.hand_on(place(deep - 1))
    loop(0, deep, settle)
    loop(0, n, rows_spread.drain)
    all_in([lower])
    keeping[2].start()

    def returning(zs, row, mine):
        return remote(
            passed.at[zs, row],
            results.at[zs, mine],
            result_send.at[zs, row],
            result_recv.at[zs, mine],
            {"fs": z * wide + row},
        )

    def multiply(i):
        zs = place(i)
        unit_spread.arrive(zs)
        for e in range(keep):
            out = jnp.dot(
                hidden[e, span(zs, group), :], held_down[e], preferred_element_type=jnp.float32
            ).astype(jnp.bfloat16)
            for row in range(wide):
                part = out[row * capacity : (row + 1) * capacity]

                @pl.when(row == y)
                def _():
                    results[zs, row, e] = part

                @pl.when(row != y)
                def _():
                    passed[zs, row, e] = part

        others(lambda row: returning(zs, row, y).start())

    def add_up(zs):
        others(lambda row: returning(zs, row, row).wait_recv())
        for row in range(wide):
            for e in range(keep):
                slot, weight = entry_slot(zs, (z * wide + row) * keep + e)
                at = (row * keep + e) * capacity
                spread_weight[at : at + capacity, :] = jnp.where(slots == slot, weight, 0.0).astype(jnp.bfloat16)
        total[...] = lax.dot_general(
            spread_weight[...],
            results[zs].reshape(wide * keep * capacity, width),
            (((0,), (0,)), ((), ())),
            preferred_element_type=jnp.float32,
        )

    def part_copy(zs, side):
        last = zs == z + side
        at = jnp.where(last & (side < 0), deep, zs)
        return remote(token.at[zs], arrived.at[at], part_send.at[zs], part_recv.at[at], {"fs": me + side * wide})

    def part_in(at):
        return remote(token.at[0], arrived.at[at], part_send.at[0], part_recv.at[at], {"fs": me})

    def toward(zs):
        return jnp.where(zs > z, 1, -1)

    def send_part(i):
        zs = place(i)
        add_up(zs)
        fed = jnp.where(zs > z, z > 0, z < deep - 1)

        @pl.when(fed)
        def _():
            part_in(zs).wait_recv()
            token[zs] = (total[...] + arrived[zs].astype(jnp.float32)).astype(jnp.bfloat16)

        @pl.when(jnp.logical_not(fed))
        def _():
            token[zs] = total[...].astype(jnp.bfloat16)

        part_copy(zs, toward(zs)).start()

    multiply(0)

    def turn_back(i):
        multiply(i)
        send_part(i - 1)

    loop(1, deep, turn_back)
    add_up(z)

    @pl.when(z > 0)
    def _():
        part_in(z).wait_recv()
        total[...] += arrived[z].astype(jnp.float32)

    @pl.when(z < deep - 1)
    def _():
        part_in(deep).wait_recv()
        total[...] += arrived[deep].astype(jnp.float32)

    mixed[...] = total[...].astype(jnp.bfloat16)
    write = pltpu.make_async_copy(mixed, mixed_out, out_sem.at[3])
    write.start()

    def sent(turn):
        for part in [*pair, lower]:
            part.copy(turn, peer(turn)).wait_send()

    loop(0, n - 1, sent)
    loop(0, deep, unit_spread.drain)

    def sent_back(i):
        zs = place(i)
        others(lambda row: returning(zs, row, y).wait_send())

        @pl.when(zs != z)
        def _():
            part_copy(zs, toward(zs)).wait_send()

    loop(0, deep, sent_back)
    for copy in keeping:
        copy.wait()
    write.wait()


def per_device(prompt, routes, affinity, norm_gain, gate_master, up_master, down_master):
    n, tp = lax.axis_size("fs"), lax.axis_size("tp")
    chips = tp // 2
    deep = n // chips if n % chips == 0 else n
    wide = n // deep
    experts, rows, units = gate_master.shape
    _, unit_rows, width = down_master.shape
    tokens, model = prompt.shape
    keep = experts // n
    capacity = 2 * tokens * routes.shape[1] // experts
    inside, anywhere = pl.BlockSpec(memory_space=pltpu.VMEM), pl.BlockSpec(memory_space=pl.ANY)
    half, full = jnp.bfloat16, jnp.float32
    dma = pltpu.SemaphoreType.DMA
    mixed, gate_new, up_new, down_new = pl.pallas_call(
        functools.partial(kernel, n, tp, deep),
        out_shape=[
            jax.ShapeDtypeStruct((tokens, width), half),
            jax.ShapeDtypeStruct((keep, model, units), half),
            jax.ShapeDtypeStruct((keep, model, units), half),
            jax.ShapeDtypeStruct((keep, unit_rows * n, width), half),
        ],
        in_specs=[inside] * 3 + [anywhere] * 4,
        out_specs=[anywhere] * 4,
        scratch_shapes=[
            pltpu.VMEM((RING, keep, rows, units), full),
            pltpu.VMEM((RING, keep, rows, units), full),
            pltpu.VMEM((RING, keep, unit_rows, width), full),
            pltpu.VMEM((n - 1, keep, rows, units), half),
            pltpu.VMEM((n - 1, keep, rows, units), half),
            pltpu.VMEM((n - 1, keep, unit_rows, width), half),
            pltpu.VMEM((keep, model, 2 * units), half),
            pltpu.VMEM((keep, unit_rows * n, width), half),
            pltpu.VMEM((tokens, model), half),
            pltpu.VMEM((deep, tokens, width), half),
            pltpu.VMEM((deep, 8, tokens), full),
            pltpu.VMEM((keep, n * capacity, model), half),
            pltpu.VMEM((deep, wide, keep, capacity, width), half),
            pltpu.VMEM((keep, n * capacity, units * tp), half),
            pltpu.VMEM((deep, wide, keep, capacity, width), half),
            pltpu.VMEM((deep + 1, tokens, width), half),
            pltpu.VMEM((tokens, width), half),
            pltpu.VMEM((wide * keep * capacity, tokens), half),
            pltpu.VMEM((tokens, width), full),
            dma((3, RING)),
            dma((3, n)),
            dma((3, n)),
            dma((1,)),
            dma((deep, 2)),
            dma((deep,)),
            dma((deep, 2)),
            dma((deep,)),
            dma((deep, wide)),
            dma((n,)),
            dma((deep, wide)),
            dma((deep, wide)),
            dma((deep,)),
            dma((deep + 1,)),
            dma((4,)),
            *[dma((n, chips))] * 4,
            *[dma((deep, chips))] * 4,
        ],
        compiler_params=pltpu.CompilerParams(
            collective_id=0, has_side_effects=True, vmem_limit_bytes=63 * 2**20
        ),
        name="experts",
    )(norm_gain[:, None], routes.T, affinity.T, prompt, gate_master, up_master, down_master)
    return (mixed, gate_new, up_new, down_new)


def solution(mesh):
    in_specs = (
        P("fs", None),
        P("fs", None),
        P("fs", None),
        P("fs"),
        P(None, "fs", "tp"),
        P(None, "fs", "tp"),
        P(None, "fs", "tp"),
    )
    out_specs = (P("fs", "tp"), P("fs", None, "tp"), P("fs", None, "tp"), P("fs", None, "tp"))
    return jax.shard_map(
        per_device, mesh=mesh, in_specs=in_specs, out_specs=out_specs, check_vma=False
    )
```

time: 319 us -> 276 us (0.87)
  the two profiles are of different devices: /device:TPU:28 before, /device:TPU:0 now
where the time goes in v1:
time: 276 us
  Pallas kernels  265 us (96%)
  local copies, waits for them, and re-layouts  10.4 us (4%)
    pallas_call x1, Pallas kernels, per_device(): pl.pallas_call(functools.partial(kernel, n, tp, deep), out_shape=[jax.Sha...  265 us
    unnamed x8, local copies, waits for them, and re-layouts  8.93 us

profile of v1, /device:TPU:0, one launch (start us, length us, event | category | flops | bytes accessed | tf_op | source)
XLA Modules:
  0.0 276.2 jit_solution(5979893827716061367)
XLA Ops:
  0.6 1.5 copy.11.gain
  2.1 265.1 %experts.1 = (bf16[768,512]{1,0:T(8,128)(2,1)}, bf16[2,2048,256]{2,1,0:T(8,128)(2,1)}, bf16[2,2048,256]{2,1,0:T(8,128)(2,1)}, bf16[2,1024,512]{2,1,0:T(8,128)(2,1)}) custom-call(f32[256,1]{1,0:T(8,128)} %copy.11.gain, s32[2,768]{1,0:T(2,128)} %bitcast.3, f32[2,768]{1,0:T(2,128)} %bitcast.4, bf16[768,2048]{1,0:T(8,128)(2,1)} %prompt.1, f32[16,256,256]{2,1,0:T(8,128)} %gate.1, ...), custom_call_target="tpu_custom_call" | custom-call | tf_op jit(solution)/shard_map/experts/pallas_call | solution.py:562
  267.2 2.1 copy.16
  269.3 0.0 copy-start.1
  269.3 3.2 %copy.17 = bf16[2,2048,256]{2,1,0:T(8,128)(2,1)} copy(bf16[2,2048,256]{2,1,0:T(8,128)(2,1)} %get-tuple-element.9) | data formatting | bytes 4194304
  272.5 0.0 copy-done.1
  272.5 0.0 copy-start
  272.5 1.3 copy.18
  273.8 1.0 copy-done
  274.9 1.3 copy.19
Async XLA Ops:
  269.3 3.2 %copy-start.1 = (bf16[2,2048,256]{2,1,0:T(8,128)(2,1)S(1)}, bf16[2,2048,256]{2,1,0:T(8,128)(2,1)}, u32[]{:S(2)}) copy-start(bf16[2,2048,256]{2,1,0:T(8,128)(2,1)} %get-tuple-element.10) | copy-start | bytes 6291460
  272.5 2.3 copy-start

commit v2 on v1

--- a/solution.py
+++ b/solution.py
@@ -10,6 +10,7 @@
 norm_eps = 1e-06
 MESH = pl.DeviceIdType.MESH
 RING = 4
+HALVES = 2
 
 
 def remote(src, dst, send_sem, recv_sem, where):
@@ -41,9 +42,22 @@
     reach = jnp.minimum(low, high)
     j = i - skew
     distance = reach - j // 2
-    paired = jnp.where(j % 2 == 0, z + distance, z - distance)
+    paired = jnp.where((j % 2 == 0) == (low < high), z + distance, z - distance)
     single = jnp.where(low > high, i, depth - 1 - i)
     return jnp.where(i < skew, single, paired)
+
+
+def giving_order(z, depth, i):
+    left = z < depth - 1 - z
+    outer = jnp.minimum(z, depth - 1 - z)
+    own = 2 * outer + 1
+    k = jnp.where(outer == 0, i - 1, i)
+    j = jnp.where(k >= own, k + 1, k)
+    inward = j // 2
+    position = jnp.where((j % 2 == 0) == left, depth - 1 - inward, inward)
+    beside = jnp.where(left, z + 1, z - 1)
+    position = jnp.where((outer == 0) & (i == 0), beside, position)
+    return jnp.where(i == depth - 1, z, position)
 
 
 class Spread:
@@ -97,11 +111,13 @@
 
 
 class Weights:
-    def __init__(self, n, master, gain, held, raw, send, load_sem, send_sem, recv_sem):
+    def __init__(self, n, master, gain, held, raw, send, load_sem, send_sem, recv_sem, cuts):
         self.n, self.master, self.gain, self.held, self.raw, self.send = n, master, gain, held, raw, send
         self.load_sem, self.send_sem, self.recv_sem = load_sem, send_sem, recv_sem
         self.keep, self.rows = master.shape[0] // n, master.shape[1]
         self.me = lax.axis_index("fs")
+        size = master.shape[2] // cuts
+        self.cuts = [slice(i * size, (i + 1) * size) for i in range(cuts)]
 
     def load(self, turn, peer):
         slot = lax.rem(turn, RING)
@@ -124,14 +140,25 @@
     def keep_own(self, turn):
         self.held[:, span(self.me, self.rows), :] = self.taken(turn)
 
-    def copy(self, turn, peer):
+    def copies(self, turn, peer, cuts=(0, 1)):
+        for cut in cuts[: len(self.cuts)]:
+            part = self.cuts[cut]
+            yield remote(
+                self.send.at[turn, :, :, part],
+                self.place(self.me).at[:, :, part],
+                self.send_sem.at[peer, cut],
+                self.recv_sem.at[self.me, cut],
+                {"fs": peer},
+            )
+
+    def arrival(self, source, cut):
+        part = self.cuts[cut]
         return remote(
-            self.send.at[turn], self.place(self.me), self.send_sem.at[peer], self.recv_sem.at[self.me], {"fs": peer}
-        )
-
-    def arrival(self, source):
-        return remote(
-            self.send.at[0], self.place(source), self.send_sem.at[source], self.recv_sem.at[source], {"fs": source}
+            self.send.at[0, :, :, part],
+            self.place(source).at[:, :, part],
+            self.send_sem.at[source, cut],
+            self.recv_sem.at[source, cut],
+            {"fs": source},
         )
 
 
@@ -200,17 +227,19 @@
     pair = [
         Weights(
             n, master, gain, held_pair.at[:, :, i * units : (i + 1) * units], raw, send,
-            load_sem.at[i], weight_send.at[i], weight_recv.at[i],
+            load_sem.at[i], weight_send.at[i], weight_recv.at[i], 1,
         )
         for i, (master, raw, send) in enumerate([(gate, raw_gate, send_gate), (up, raw_up, send_up)])
     ]
-    lower = Weights(n, down, None, held_down, raw_down, send_down, load_sem.at[2], weight_send.at[2], weight_recv.at[2])
+    lower = Weights(
+        n, down, None, held_down, raw_down, send_down, load_sem.at[2], weight_send.at[2], weight_recv.at[2], HALVES
+    )
 
     def place(i):
         return far_first(z, deep, i)
 
     def peer(turn):
-        return place(turn // wide) * wide + lax.rem(y + 1 + lax.rem(turn, wide), wide)
+        return giving_order(z, deep, turn // wide) * wide + lax.rem(y + 1 + lax.rem(turn, wide), wide)
 
     barrier = pltpu.get_barrier_semaphore()
     for step in range(1, n):
@@ -246,6 +275,25 @@
         ],
         axis=0,
     )
+    def give_weights(parts, first, last, cuts=(0, 1)):
+        def body(turn):
+            target = peer(turn)
+            for part in parts:
+                if 0 in cuts:
+                    part.load(turn, target).wait()
+                    part.cast(turn)
+
+                    @pl.when(turn + RING < n)
+                    def _():
+                        part.load(turn + RING, peer(turn + RING)).start()
+
+                for copy in part.copies(turn, target, cuts):
+                    copy.start()
+
+        loop(first, last, body)
+
+    pl.semaphore_wait(barrier, n - 1 + rows_spread.chips)
+    give_weights(pair[:1], 0, 1)
     fetch.wait()
     tile = 128
 
@@ -256,7 +304,6 @@
         token[z, rows, :] = (prompt_in[rows, column].astype(jnp.float32) * scale).astype(jnp.bfloat16)
 
     loop(0, tokens // tile, normalize)
-    pl.semaphore_wait(barrier, n - 1 + rows_spread.chips)
 
     def onward(zs, side):
         where = {"fs": me + side * wide}
@@ -337,23 +384,29 @@
     def hand_on_passed(zs):
         others(lambda row: rows_spread.hand_on(zs * wide + row))
 
-    def give_weights(parts, first, last):
-        def body(turn):
-            target = peer(turn)
-            for part in parts:
-                part.load(turn, target).wait()
-                part.cast(turn)
-
-                @pl.when(turn + RING < n)
-                def _():
-                    part.load(turn + RING, peer(turn + RING)).start()
-
-                part.copy(turn, target).start()
-
-        loop(first, last, body)
+    end = (z == 0) | (z == deep - 1)
+    to_line = (deep - 1) * wide
+
+    def give_from_end():
+        give_weights(pair[1:], 0, 1)
+        give_weights(pair, 1, wide)
+        give_weights([lower], 0, wide)
+        give_weights(pair, wide, to_line)
+        give_weights([lower], wide, to_line)
+
+    def give_far():
+        give_weights(pair[1:], 0, 1)
+        give_weights(pair, 1, wide)
+
+    def give_rest():
+        give_weights(pair, wide, to_line)
+        give_weights([lower], 0, 2 * wide)
+        for cut in range(HALVES):
+            give_weights([lower], 2 * wide, to_line, (cut,))
 
     sends(z, lambda copy: copy.start())
     extract(z)
+    pl.when(end)(give_from_end)
 
     def hop(i):
         zs = near_first(i)
@@ -361,6 +414,8 @@
             copy.wait_recv()
         sends(zs, lambda copy: copy.start())
         extract(zs)
+        pl.when(jnp.logical_not(end) & (i == deep - 2))(give_far)
+        pl.when(jnp.logical_not(end) & (i == deep - 1))(give_rest)
         before = near_first(i - 1)
         take_passed(before)
         rows_spread.hand_on(before * wide + y)
@@ -369,36 +424,32 @@
         def _():
             hand_on_passed(near_first(i - 2))
 
-        first = jnp.where(i == 1, 0, (i - 1) * (n - 1) // deep)
-        last = i * (n - 1) // deep
-        give_weights(pair, first, last)
-
     loop(1, deep, hop)
-    give_weights(pair, (deep - 1) * (n - 1) // deep, n - 1)
     final = near_first(deep - 1)
-    take_passed(final)
-    hand_on_passed(near_first(deep - 2))
-    give_weights([lower], 0, n - 1)
-    rows_spread.hand_on(final * wide + y)
-    hand_on_passed(final)
+    give_weights(pair, to_line, n - 1)
+    give_weights([lower], to_line, n - 1)
     for part in [*pair, lower]:
         part.load(n - 1, me).wait()
         part.keep_own(n - 1)
+    rows_spread.hand_on(final * wide + y)
+    hand_on_passed(near_first(deep - 2))
+    take_passed(final)
+    hand_on_passed(final)
     loop(0, n, rows_spread.arrive)
 
     def settle(zs):
         sends(zs, lambda copy: copy.wait_send())
         others(lambda row: passing(zs, row).wait_send())
 
-    def all_in(parts):
+    def all_in(parts, cut):
         def body(step):
             source = lax.rem(me + step, n)
             for part in parts:
-                part.arrival(source).wait_recv()
+                part.arrival(source, cut).wait_recv()
 
         loop(1, n, body)
 
-    all_in(pair)
+    all_in(pair, 0)
     keeping = [
         pltpu.make_async_copy(held_pair.at[:, :, :units], gate_out, out_sem.at[0]),
         pltpu.make_async_copy(held_pair.at[:, :, units:], up_out, out_sem.at[1]),
@@ -429,40 +480,41 @@
     unit_spread.hand_on(place(deep - 1))
     loop(0, deep, settle)
     loop(0, n, rows_spread.drain)
-    all_in([lower])
-    keeping[2].start()
-
-    def returning(zs, row, mine):
+
+    half = width // HALVES
+
+    def columns(cut):
+        return slice(cut * half, (cut + 1) * half)
+
+    def returning(zs, row, mine, cut):
         return remote(
-            passed.at[zs, row],
-            results.at[zs, mine],
-            result_send.at[zs, row],
-            result_recv.at[zs, mine],
+            passed.at[zs, row, :, :, columns(cut)],
+            results.at[zs, mine, :, :, columns(cut)],
+            result_send.at[zs, row, cut],
+            result_recv.at[zs, mine, cut],
             {"fs": z * wide + row},
         )
 
-    def multiply(i):
-        zs = place(i)
-        unit_spread.arrive(zs)
+    def multiply(zs, cut):
         for e in range(keep):
             out = jnp.dot(
-                hidden[e, span(zs, group), :], held_down[e], preferred_element_type=jnp.float32
+                hidden[e, span(zs, group), :], held_down[e, :, columns(cut)], preferred_element_type=jnp.float32
             ).astype(jnp.bfloat16)
             for row in range(wide):
                 part = out[row * capacity : (row + 1) * capacity]
 
                 @pl.when(row == y)
                 def _():
-                    results[zs, row, e] = part
+                    results[zs, row, e, :, columns(cut)] = part
 
                 @pl.when(row != y)
                 def _():
-                    passed[zs, row, e] = part
-
-        others(lambda row: returning(zs, row, y).start())
-
-    def add_up(zs):
-        others(lambda row: returning(zs, row, row).wait_recv())
+                    passed[zs, row, e, :, columns(cut)] = part
+
+        others(lambda row: returning(zs, row, y, cut).start())
+
+    def add_up(zs, cut):
+        others(lambda row: returning(zs, row, row, cut).wait_recv())
         for row in range(wide):
             for e in range(keep):
                 slot, weight = entry_slot(zs, (z * wide + row) * keep + e)
@@ -470,80 +522,113 @@
                 spread_weight[at : at + capacity, :] = jnp.where(slots == slot, weight, 0.0).astype(jnp.bfloat16)
         total[...] = lax.dot_general(
             spread_weight[...],
-            results[zs].reshape(wide * keep * capacity, width),
+            results[zs, :, :, :, columns(cut)].reshape(wide * keep * capacity, half),
             (((0,), (0,)), ((), ())),
             preferred_element_type=jnp.float32,
         )
 
-    def part_copy(zs, side):
+    def part_copy(zs, side, cut):
         last = zs == z + side
         at = jnp.where(last & (side < 0), deep, zs)
-        return remote(token.at[zs], arrived.at[at], part_send.at[zs], part_recv.at[at], {"fs": me + side * wide})
-
-    def part_in(at):
-        return remote(token.at[0], arrived.at[at], part_send.at[0], part_recv.at[at], {"fs": me})
+        return remote(
+            token.at[zs, :, columns(cut)],
+            arrived.at[at, :, columns(cut)],
+            part_send.at[zs, cut],
+            part_recv.at[at, cut],
+            {"fs": me + side * wide},
+        )
+
+    def part_in(at, cut):
+        return remote(
+            token.at[0, :, columns(cut)],
+            arrived.at[at, :, columns(cut)],
+            part_send.at[0, cut],
+            part_recv.at[at, cut],
+            {"fs": me},
+        )
 
     def toward(zs):
         return jnp.where(zs > z, 1, -1)
 
-    def send_part(i):
-        zs = place(i)
-        add_up(zs)
+    def send_part(zs, cut):
+        add_up(zs, cut)
         fed = jnp.where(zs > z, z > 0, z < deep - 1)
 
         @pl.when(fed)
         def _():
-            part_in(zs).wait_recv()
-            token[zs] = (total[...] + arrived[zs].astype(jnp.float32)).astype(jnp.bfloat16)
+            part_in(zs, cut).wait_recv()
+            token[zs, :, columns(cut)] = (
+                total[...] + arrived[zs, :, columns(cut)].astype(jnp.float32)
+            ).astype(jnp.bfloat16)
 
         @pl.when(jnp.logical_not(fed))
         def _():
-            token[zs] = total[...].astype(jnp.bfloat16)
-
-        part_copy(zs, toward(zs)).start()
-
-    multiply(0)
-
-    def turn_back(i):
-        multiply(i)
-        send_part(i - 1)
-
-    loop(1, deep, turn_back)
-    add_up(z)
-
-    @pl.when(z > 0)
-    def _():
-        part_in(z).wait_recv()
-        total[...] += arrived[z].astype(jnp.float32)
-
-    @pl.when(z < deep - 1)
-    def _():
-        part_in(deep).wait_recv()
-        total[...] += arrived[deep].astype(jnp.float32)
-
-    mixed[...] = total[...].astype(jnp.bfloat16)
-    write = pltpu.make_async_copy(mixed, mixed_out, out_sem.at[3])
-    write.start()
+            token[zs, :, columns(cut)] = total[...].astype(jnp.bfloat16)
+
+        part_copy(zs, toward(zs), cut).start()
+
+    def first_half(i):
+        unit_spread.arrive(place(i))
+        multiply(place(i), 0)
+
+    all_in([lower], 0)
+    first_half(0)
+
+    def overlap(i):
+        first_half(i)
+        send_part(place(i - 1), 0)
+
+    loop(1, deep - 1, overlap)
+    first_half(deep - 1)
+    for cut in range(1, HALVES):
+        all_in([lower], cut)
+        if cut == HALVES - 1:
+            keeping[2].start()
+        loop(0, deep, lambda i: multiply(place(i), cut))
+        send_part(place(deep - 2), cut - 1)
+        loop(0, deep - 2, lambda i: send_part(place(i), cut))
+    send_part(place(deep - 2), HALVES - 1)
+    writes = []
+    for cut in range(HALVES):
+        add_up(z, cut)
+
+        @pl.when(z > 0)
+        def _():
+            part_in(z, cut).wait_recv()
+            total[...] += arrived[z, :, columns(cut)].astype(jnp.float32)
+
+        @pl.when(z < deep - 1)
+        def _():
+            part_in(deep, cut).wait_recv()
+            total[...] += arrived[deep, :, columns(cut)].astype(jnp.float32)
+
+        mixed[:, columns(cut)] = total[...].astype(jnp.bfloat16)
+        write = pltpu.make_async_copy(
+            mixed.at[:, columns(cut)], mixed_out.at[:, columns(cut)], out_sem.at[3 + cut]
+        )
+        write.start()
+        writes.append(write)
 
     def sent(turn):
         for part in [*pair, lower]:
-            part.copy(turn, peer(turn)).wait_send()
+            for copy in part.copies(turn, peer(turn)):
+                copy.wait_send()
 
     loop(0, n - 1, sent)
     loop(0, deep, unit_spread.drain)
 
     def sent_back(i):
         zs = place(i)
-        others(lambda row: returning(zs, row, y).wait_send())
-
-        @pl.when(zs != z)
-        def _():
-            part_copy(zs, toward(zs)).wait_send()
+        for cut in range(HALVES):
+            others(lambda row: returning(zs, row, y, cut).wait_send())
+
+            @pl.when(zs != z)
+            def _():
+                part_copy(zs, toward(zs), cut).wait_send()
 
     loop(0, deep, sent_back)
-    for copy in keeping:
+    for copy in [*keeping, *writes]:
         copy.wait()
-    write.wait()
 
 
 def per_device(prompt, routes, affinity, norm_gain, gate_master, up_master, down_master):
@@ -588,10 +673,10 @@
             pltpu.VMEM((deep + 1, tokens, width), half),
             pltpu.VMEM((tokens, width), half),
             pltpu.VMEM((wide * keep * capacity, tokens), half),
-            pltpu.VMEM((tokens, width), full),
+            pltpu.VMEM((tokens, width // HALVES), full),
             dma((3, RING)),
-            dma((3, n)),
-            dma((3, n)),
+            dma((3, n, HALVES)),
+            dma((3, n, HALVES)),
             dma((1,)),
             dma((deep, 2)),
             dma((deep,)),
@@ -599,11 +684,11 @@
             dma((deep,)),
             dma((deep, wide)),
             dma((n,)),
-            dma((deep, wide)),
-            dma((deep, wide)),
-            dma((deep,)),
-            dma((deep + 1,)),
-            dma((4,)),
+            dma((deep, wide, HALVES)),
+            dma((deep, wide, HALVES)),
+            dma((deep, HALVES)),
+            dma((deep + 1, HALVES)),
+            dma((3 + HALVES,)),
             *[dma((n, chips))] * 4,
             *[dma((deep, chips))] * 4,
         ],

time: 276 us -> 248 us (0.90)
  Pallas kernels: 265 us -> 236 us
    pallas_call x1, Pallas kernels: 265 us -> 236 us  [per_device(): pl.pallas_call(functools.partial(kernel, n, tp, deep), out_shape=[jax.Sha...]
where the time goes in v2:
time: 248 us; the launch traced here: 247 us
  Pallas kernels  236 us (95%)
  local copies, waits for them, and re-layouts  10.4 us (4%)
    pallas_call x1, Pallas kernels, per_device(): pl.pallas_call(functools.partial(kernel, n, tp, deep), out_shape=[jax.Sha...  236 us
    unnamed x8, local copies, waits for them, and re-layouts  8.93 us

profile of v2, /device:TPU:0, one launch (start us, length us, event | category | flops | bytes accessed | tf_op | source)
XLA Modules:
  0.0 247.4 jit_solution(5678553906070949332)
XLA Ops:
  0.6 1.5 copy.11.gain
  2.1 236.4 %experts.1 = (bf16[768,512]{1,0:T(8,128)(2,1)}, bf16[2,2048,256]{2,1,0:T(8,128)(2,1)}, bf16[2,2048,256]{2,1,0:T(8,128)(2,1)}, bf16[2,1024,512]{2,1,0:T(8,128)(2,1)}) custom-call(f32[256,1]{1,0:T(8,128)} %copy.11.gain, s32[2,768]{1,0:T(2,128)} %bitcast.3, f32[2,768]{1,0:T(2,128)} %bitcast.4, bf16[768,2048]{1,0:T(8,128)(2,1)} %prompt.1, f32[16,256,256]{2,1,0:T(8,128)} %gate.1, ...), custom_call_target="tpu_custom_call" | custom-call | tf_op jit(solution)/shard_map/experts/pallas_call | solution.py:647
  238.5 2.1 copy.16
  240.5 0.0 copy-start.1
  240.5 3.2 %copy.17 = bf16[2,2048,256]{2,1,0:T(8,128)(2,1)} copy(bf16[2,2048,256]{2,1,0:T(8,128)(2,1)} %get-tuple-element.9) | data formatting | bytes 4194304
  243.7 0.0 copy-done.1
  243.7 0.0 copy-start
  243.7 1.3 copy.18
  245.1 1.0 copy-done
  246.1 1.3 copy.19
Async XLA Ops:
  240.5 3.2 %copy-start.1 = (bf16[2,2048,256]{2,1,0:T(8,128)(2,1)S(1)}, bf16[2,2048,256]{2,1,0:T(8,128)(2,1)}, u32[]{:S(2)}) copy-start(bf16[2,2048,256]{2,1,0:T(8,128)(2,1)} %get-tuple-element.10) | copy-start | bytes 6291460
  243.7 2.3 copy-start

commit v3 on v2

--- a/solution.py
+++ b/solution.py
@@ -51,18 +51,18 @@
     left = z < depth - 1 - z
     outer = jnp.minimum(z, depth - 1 - z)
     own = 2 * outer + 1
-    k = jnp.where(outer == 0, i - 1, i)
-    j = jnp.where(k >= own, k + 1, k)
+    j = jnp.where(i >= own, i + 1, i)
     inward = j // 2
     position = jnp.where((j % 2 == 0) == left, depth - 1 - inward, inward)
-    beside = jnp.where(left, z + 1, z - 1)
-    position = jnp.where((outer == 0) & (i == 0), beside, position)
+    outwards = jnp.where(left, i + 1, depth - 2 - i)
+    position = jnp.where(outer == 0, outwards, position)
     return jnp.where(i == depth - 1, z, position)
 
 
 class Spread:
-    def __init__(self, tp, whole, rows, width, sems):
+    def __init__(self, tp, whole, rows, width, sems, groups=None):
         self.chips = tp // 2
+        self.groups = groups
         self.me = lax.axis_index("tp")
         self.chip, self.core = self.me // 2, self.me % 2
         self.whole, self.rows, self.width = whole, rows, width
@@ -74,7 +74,10 @@
         return lax.rem(self.chip + hop, self.chips) * 2 + self.core
 
     def block(self, chunk, owner):
-        return self.whole.at[:, span(chunk, self.rows), span(owner, self.width)]
+        if self.groups is None:
+            return self.whole.at[:, span(chunk, self.rows), span(owner, self.width)]
+        rows = span(lax.rem(chunk, self.groups), self.rows)
+        return self.whole.at[chunk // self.groups, rows, span(owner, self.width)]
 
     def first(self, chunk, hop):
         mine = self.block(chunk, self.me)
@@ -116,8 +119,11 @@
         self.load_sem, self.send_sem, self.recv_sem = load_sem, send_sem, recv_sem
         self.keep, self.rows = master.shape[0] // n, master.shape[1]
         self.me = lax.axis_index("fs")
-        size = master.shape[2] // cuts
-        self.cuts = [slice(i * size, (i + 1) * size) for i in range(cuts)]
+        if cuts is None:
+            self.cuts = [(slice(e, e + 1), slice(None)) for e in range(self.keep)]
+        else:
+            size = master.shape[2] // cuts
+            self.cuts = [(slice(None), slice(i * size, (i + 1) * size)) for i in range(cuts)]
 
     def load(self, turn, peer):
         slot = lax.rem(turn, RING)
@@ -140,22 +146,22 @@
     def keep_own(self, turn):
         self.held[:, span(self.me, self.rows), :] = self.taken(turn)
 
-    def copies(self, turn, peer, cuts=(0, 1)):
-        for cut in cuts[: len(self.cuts)]:
-            part = self.cuts[cut]
+    def copies(self, turn, peer, cuts=None):
+        for cut in range(len(self.cuts)) if cuts is None else cuts:
+            one, part = self.cuts[cut]
             yield remote(
-                self.send.at[turn, :, :, part],
-                self.place(self.me).at[:, :, part],
+                self.send.at[turn, one, :, part],
+                self.place(self.me).at[one, :, part],
                 self.send_sem.at[peer, cut],
                 self.recv_sem.at[self.me, cut],
                 {"fs": peer},
             )
 
     def arrival(self, source, cut):
-        part = self.cuts[cut]
+        one, part = self.cuts[cut]
         return remote(
-            self.send.at[0, :, :, part],
-            self.place(source).at[:, :, part],
+            self.send.at[0, one, :, part],
+            self.place(source).at[one, :, part],
             self.send_sem.at[source, cut],
             self.recv_sem.at[source, cut],
             {"fs": source},
@@ -166,25 +172,22 @@
     n,
     tp,
     deep,
-    gain,
+    gain_row,
     routes,
     affinity,
     prompt,
     gate,
     up,
     down,
-    mixed_out,
-    gate_out,
-    up_out,
-    down_out,
+    mixed,
+    held_pair,
+    held_down,
     raw_gate,
     raw_up,
     raw_down,
     send_gate,
     send_up,
     send_down,
-    held_pair,
-    held_down,
     prompt_in,
     token,
     info,
@@ -193,9 +196,9 @@
     hidden,
     results,
     arrived,
-    mixed,
     spread_weight,
     total,
+    gain,
     load_sem,
     weight_send,
     weight_recv,
@@ -210,7 +213,6 @@
     result_recv,
     part_send,
     part_recv,
-    out_sem,
     *spreads,
 ):
     wide = n // deep
@@ -223,11 +225,11 @@
     column = span(lax.axis_index("tp"), width)
 
     rows_spread = Spread(tp, gathered, capacity, width, spreads[:4])
-    unit_spread = Spread(tp, hidden, wide * capacity, units, spreads[4:])
+    unit_spread = Spread(tp, hidden, wide * capacity, units, spreads[4:], deep)
     pair = [
         Weights(
             n, master, gain, held_pair.at[:, :, i * units : (i + 1) * units], raw, send,
-            load_sem.at[i], weight_send.at[i], weight_recv.at[i], 1,
+            load_sem.at[i], weight_send.at[i], weight_recv.at[i], None,
         )
         for i, (master, raw, send) in enumerate([(gate, raw_gate, send_gate), (up, raw_up, send_up)])
     ]
@@ -251,6 +253,10 @@
     for part in [*pair, lower]:
         for turn in range(RING):
             part.load(turn, peer(turn)).start()
+
+    square = (gain.shape[0], gain.shape[0])
+    diagonal = lax.broadcasted_iota(jnp.int32, square, 0) == lax.broadcasted_iota(jnp.int32, square, 1)
+    gain[...] = jnp.sum(jnp.where(diagonal, gain_row[...], 0.0), axis=1, keepdims=True)
 
     r0, r1 = routes[0:1, :], routes[1:2, :]
     names = lax.broadcasted_iota(jnp.int32, (experts, tokens), 0)
@@ -275,11 +281,11 @@
         ],
         axis=0,
     )
-    def give_weights(parts, first, last, cuts=(0, 1)):
+    def give_weights(parts, first, last, cuts=None):
         def body(turn):
             target = peer(turn)
             for part in parts:
-                if 0 in cuts:
+                if cuts is None or 0 in cuts:
                     part.load(turn, target).wait()
                     part.cast(turn)
 
@@ -293,7 +299,8 @@
         loop(first, last, body)
 
     pl.semaphore_wait(barrier, n - 1 + rows_spread.chips)
-    give_weights(pair[:1], 0, 1)
+    end = (z == 0) | (z == deep - 1)
+    pl.when(jnp.logical_not(end))(lambda: give_weights(pair[:1], 0, 1, (0,)))
     fetch.wait()
     tile = 128
 
@@ -384,24 +391,31 @@
     def hand_on_passed(zs):
         others(lambda row: rows_spread.hand_on(zs * wide + row))
 
-    end = (z == 0) | (z == deep - 1)
     to_line = (deep - 1) * wide
 
+    rest = range(1, keep)
+
     def give_from_end():
-        give_weights(pair[1:], 0, 1)
-        give_weights(pair, 1, wide)
-        give_weights([lower], 0, wide)
-        give_weights(pair, wide, to_line)
-        give_weights([lower], wide, to_line)
+        give_weights(pair, 0, wide)
+        give_weights([lower], 0, 1)
+        give_weights(pair, wide, to_line, (0,))
+        give_weights(pair, wide, to_line, rest)
+        give_weights([lower], 1, to_line)
 
     def give_far():
-        give_weights(pair[1:], 0, 1)
-        give_weights(pair, 1, wide)
+        give_weights(pair[1:], 0, 1, (0,))
+        give_weights(pair, 1, wide, (0,))
 
     def give_rest():
-        give_weights(pair, wide, to_line)
-        give_weights([lower], 0, 2 * wide)
-        for cut in range(HALVES):
+        give_weights(pair, wide, 2 * wide)
+        give_weights(pair, 2 * wide, to_line, (0,))
+        give_weights(pair, 0, wide, rest)
+        give_weights([lower], 0, wide, (0,))
+        give_weights([lower], wide, 2 * wide)
+        give_weights(pair, 2 * wide, to_line, rest)
+        give_weights([lower], 2 * wide, to_line, (0,))
+        for cut in range(1, HALVES):
+            give_weights([lower], 0, wide, (cut,))
             give_weights([lower], 2 * wide, to_line, (cut,))
 
     sends(z, lambda copy: copy.start())
@@ -449,37 +463,29 @@
 
         loop(1, n, body)
 
-    all_in(pair, 0)
-    keeping = [
-        pltpu.make_async_copy(held_pair.at[:, :, :units], gate_out, out_sem.at[0]),
-        pltpu.make_async_copy(held_pair.at[:, :, units:], up_out, out_sem.at[1]),
-        pltpu.make_async_copy(held_down, down_out, out_sem.at[2]),
-    ]
-    keeping[0].start()
-    keeping[1].start()
     unit_column = span(lax.axis_index("tp"), units)
     group = wide * capacity
 
-    def produce(i):
-        zs = place(i)
-        for e in range(keep):
+    def produce(e):
+        all_in(pair, e)
+
+        def body(i):
+            zs = place(i)
             both = jnp.dot(gathered[e, span(zs, group), :], held_pair[e], preferred_element_type=jnp.float32)
             gate_pre, up_pre = both[:, :units], both[:, units:]
             hidden[e, span(zs, group), unit_column] = (
                 gate_pre / (1.0 + jnp.exp(-gate_pre)) * up_pre
             ).astype(jnp.bfloat16)
-        unit_spread.start(zs)
-
-    produce(0)
-
-    def advance(i):
-        produce(i)
-        unit_spread.hand_on(place(i - 1))
-
-    loop(1, deep, advance)
-    unit_spread.hand_on(place(deep - 1))
+            unit_spread.start(e * deep + zs)
+
+        loop(0, deep, body)
+
+    for e in range(keep - 1):
+        produce(e)
+        loop(0, deep, lambda i: unit_spread.hand_on(e * deep + place(i)))
     loop(0, deep, settle)
     loop(0, n, rows_spread.drain)
+    produce(keep - 1)
 
     half = width // HALVES
 
@@ -567,28 +573,30 @@
 
         part_copy(zs, toward(zs), cut).start()
 
-    def first_half(i):
-        unit_spread.arrive(place(i))
-        multiply(place(i), 0)
-
+    def enter(i):
+        unit_spread.hand_on((keep - 1) * deep + place(i))
+        for e in range(keep):
+            unit_spread.arrive(e * deep + place(i))
+
+    enter(0)
     all_in([lower], 0)
-    first_half(0)
-
-    def overlap(i):
-        first_half(i)
-        send_part(place(i - 1), 0)
-
-    loop(1, deep - 1, overlap)
-    first_half(deep - 1)
+    multiply(place(0), 0)
+
+    def turn_back(i):
+        enter(i + 1)
+        multiply(place(i + 1), 0)
+
+        @pl.when(i < deep - 2)
+        def _():
+            send_part(place(i), 0)
+
+    loop(0, deep - 1, turn_back)
     for cut in range(1, HALVES):
         all_in([lower], cut)
-        if cut == HALVES - 1:
-            keeping[2].start()
         loop(0, deep, lambda i: multiply(place(i), cut))
         send_part(place(deep - 2), cut - 1)
         loop(0, deep - 2, lambda i: send_part(place(i), cut))
     send_part(place(deep - 2), HALVES - 1)
-    writes = []
     for cut in range(HALVES):
         add_up(z, cut)
 
@@ -603,11 +611,6 @@
             total[...] += arrived[deep, :, columns(cut)].astype(jnp.float32)
 
         mixed[:, columns(cut)] = total[...].astype(jnp.bfloat16)
-        write = pltpu.make_async_copy(
-            mixed.at[:, columns(cut)], mixed_out.at[:, columns(cut)], out_sem.at[3 + cut]
-        )
-        write.start()
-        writes.append(write)
 
     def sent(turn):
         for part in [*pair, lower]:
@@ -615,7 +618,7 @@
                 copy.wait_send()
 
     loop(0, n - 1, sent)
-    loop(0, deep, unit_spread.drain)
+    loop(0, keep * deep, unit_spread.drain)
 
     def sent_back(i):
         zs = place(i)
@@ -627,8 +630,6 @@
                 part_copy(zs, toward(zs), cut).wait_send()
 
     loop(0, deep, sent_back)
-    for copy in [*keeping, *writes]:
-        copy.wait()
 
 
 def per_device(prompt, routes, affinity, norm_gain, gate_master, up_master, down_master):
@@ -644,16 +645,15 @@
     inside, anywhere = pl.BlockSpec(memory_space=pltpu.VMEM), pl.BlockSpec(memory_space=pl.ANY)
     half, full = jnp.bfloat16, jnp.float32
     dma = pltpu.SemaphoreType.DMA
-    mixed, gate_new, up_new, down_new = pl.pallas_call(
+    mixed, pair, down_new = pl.pallas_call(
         functools.partial(kernel, n, tp, deep),
         out_shape=[
-            jax.ShapeDtypeStruct((tokens, width), half),
-            jax.ShapeDtypeStruct((keep, model, units), half),
-            jax.ShapeDtypeStruct((keep, model, units), half),
-            jax.ShapeDtypeStruct((keep, unit_rows * n, width), half),
+            pltpu.VMEM((tokens, width), half),
+            pltpu.VMEM((keep, model, 2 * units), half),
+            pltpu.VMEM((keep, unit_rows * n, width), half),
         ],
         in_specs=[inside] * 3 + [anywhere] * 4,
-        out_specs=[anywhere] * 4,
+        out_specs=[inside] * 3,
         scratch_shapes=[
             pltpu.VMEM((RING, keep, rows, units), full),
             pltpu.VMEM((RING, keep, rows, units), full),
@@ -661,8 +661,6 @@
             pltpu.VMEM((n - 1, keep, rows, units), half),
             pltpu.VMEM((n - 1, keep, rows, units), half),
             pltpu.VMEM((n - 1, keep, unit_rows, width), half),
-            pltpu.VMEM((keep, model, 2 * units), half),
-            pltpu.VMEM((keep, unit_rows * n, width), half),
             pltpu.VMEM((tokens, model), half),
             pltpu.VMEM((deep, tokens, width), half),
             pltpu.VMEM((deep, 8, tokens), full),
@@ -671,9 +669,9 @@
             pltpu.VMEM((keep, n * capacity, units * tp), half),
             pltpu.VMEM((deep, wide, keep, capacity, width), half),
             pltpu.VMEM((deep + 1, tokens, width), half),
-            pltpu.VMEM((tokens, width), half),
             pltpu.VMEM((wide * keep * capacity, tokens), half),
             pltpu.VMEM((tokens, width // HALVES), full),
+            pltpu.VMEM((rows, 1), full),
             dma((3, RING)),
             dma((3, n, HALVES)),
             dma((3, n, HALVES)),
@@ -688,16 +686,15 @@
             dma((deep, wide, HALVES)),
             dma((deep, HALVES)),
             dma((deep + 1, HALVES)),
-            dma((3 + HALVES,)),
             *[dma((n, chips))] * 4,
-            *[dma((deep, chips))] * 4,
+            *[dma((keep * deep, chips))] * 4,
         ],
         compiler_params=pltpu.CompilerParams(
-            collective_id=0, has_side_effects=True, vmem_limit_bytes=63 * 2**20
+            collective_id=0, has_side_effects=True, vmem_limit_bytes=55 * 2**20
         ),
         name="experts",
-    )(norm_gain[:, None], routes.T, affinity.T, prompt, gate_master, up_master, down_master)
-    return (mixed, gate_new, up_new, down_new)
+    )(norm_gain[None, :], routes.T, affinity.T, prompt, gate_master, up_master, down_master)
+    return (mixed, pair[:, :, :units], pair[:, :, units:], down_new)
 
 
 def solution(mesh):

time: 248 us -> 230 us (0.927)
  Pallas kernels: 236 us -> 225 us
  local copies, waits for them, and re-layouts: 10.4 us -> 4.48 us
    pallas_call x1, Pallas kernels: 236 us -> 225 us  [per_device(): pl.pallas_call(functools.partial(kernel, n, tp, deep), out_shape=[pltpu.V...]
    unnamed x8 -> x2, local copies, waits for them, and re-layouts: 8.93 us -> 2.2 us
where the time goes in v3:
time: 230 us
  Pallas kernels  225 us (98%)
  local copies, waits for them, and re-layouts  4.48 us (2%)
    pallas_call x1, Pallas kernels, per_device(): pl.pallas_call(functools.partial(kernel, n, tp, deep), out_shape=[pltpu.V...  225 us

profile of v3, /device:TPU:0, one launch (start us, length us, event | category | flops | bytes accessed | tf_op | source)
XLA Modules:
  0.0 229.6 jit_solution(17960392463139328357)
XLA Ops:
  0.6 224.5 %experts.1 = (bf16[768,512]{1,0:T(8,128)(2,1)S(1)}, bf16[2,2048,512]{2,1,0:T(8,128)(2,1)S(1)}, bf16[2,1024,512]{2,1,0:T(8,128)(2,1)S(1)}) custom-call(f32[1,256]{1,0:T(1,128)} %bitcast.5, s32[2,768]{1,0:T(2,128)} %bitcast.3, f32[2,768]{1,0:T(2,128)} %bitcast.4, bf16[768,2048]{1,0:T(8,128)(2,1)} %prompt.1, f32[16,256,256]{2,1,0:T(8,128)} %gate.1, ...), custom_call_target="tpu_custom_call" | custom-call | tf_op jit(solution)/shard_map/experts/pallas_call | solution.py:648
  225.1 0.9 copy.13
  226.0 1.3 copy.14
  227.3 2.3 fusion

commit v4 on v3

--- a/solution.py
+++ b/solution.py
@@ -198,6 +198,7 @@
     arrived,
     spread_weight,
     total,
+    own,
     gain,
     load_sem,
     weight_send,
@@ -480,6 +481,14 @@
 
         loop(0, deep, body)
 
+    def weigh(zs):
+        for row in range(wide):
+            for e in range(keep):
+                slot, weight = entry_slot(zs, (z * wide + row) * keep + e)
+                at = (row * keep + e) * capacity
+                spread_weight[zs, at : at + capacity, :] = jnp.where(slots == slot, weight, 0.0).astype(jnp.bfloat16)
+
+    loop(0, deep, weigh)
     for e in range(keep - 1):
         produce(e)
         loop(0, deep, lambda i: unit_spread.hand_on(e * deep + place(i)))
@@ -487,10 +496,12 @@
     loop(0, n, rows_spread.drain)
     produce(keep - 1)
 
-    half = width // HALVES
+    cuts = part_send.shape[1]
+    per = cuts // HALVES
+    half, piece = width // HALVES, width // cuts
 
     def columns(cut):
-        return slice(cut * half, (cut + 1) * half)
+        return slice(cut * piece, (cut + 1) * piece)
 
     def returning(zs, row, mine, cut):
         return remote(
@@ -501,34 +512,31 @@
             {"fs": z * wide + row},
         )
 
-    def multiply(zs, cut):
+    def multiply(zs, side):
+        here = slice(side * half, (side + 1) * half)
         for e in range(keep):
             out = jnp.dot(
-                hidden[e, span(zs, group), :], held_down[e, :, columns(cut)], preferred_element_type=jnp.float32
+                hidden[e, span(zs, group), :], held_down[e, :, here], preferred_element_type=jnp.float32
             ).astype(jnp.bfloat16)
             for row in range(wide):
                 part = out[row * capacity : (row + 1) * capacity]
 
                 @pl.when(row == y)
                 def _():
-                    results[zs, row, e, :, columns(cut)] = part
+                    results[zs, row, e, :, here] = part
 
                 @pl.when(row != y)
                 def _():
-                    passed[zs, row, e, :, columns(cut)] = part
-
+                    passed[zs, row, e, :, here] = part
+
+    def give_back(zs, cut):
         others(lambda row: returning(zs, row, y, cut).start())
 
-    def add_up(zs, cut):
+    def summed(zs, cut):
         others(lambda row: returning(zs, row, row, cut).wait_recv())
-        for row in range(wide):
-            for e in range(keep):
-                slot, weight = entry_slot(zs, (z * wide + row) * keep + e)
-                at = (row * keep + e) * capacity
-                spread_weight[at : at + capacity, :] = jnp.where(slots == slot, weight, 0.0).astype(jnp.bfloat16)
-        total[...] = lax.dot_general(
-            spread_weight[...],
-            results[zs, :, :, :, columns(cut)].reshape(wide * keep * capacity, half),
+        return lax.dot_general(
+            spread_weight[zs],
+            results[zs, :, :, :, columns(cut)].reshape(wide * keep * capacity, piece),
             (((0,), (0,)), ((), ())),
             preferred_element_type=jnp.float32,
         )
@@ -557,7 +565,7 @@
         return jnp.where(zs > z, 1, -1)
 
     def send_part(zs, cut):
-        add_up(zs, cut)
+        total[...] = summed(zs, cut)
         fed = jnp.where(zs > z, z > 0, z < deep - 1)
 
         @pl.when(fed)
@@ -573,44 +581,90 @@
 
         part_copy(zs, toward(zs), cut).start()
 
+    def add_own(cut):
+        own[:, columns(cut)] = summed(z, cut)
+
+    def finish(cut):
+        @pl.when(z > 0)
+        def _():
+            part_in(z, cut).wait_recv()
+            own[:, columns(cut)] += arrived[z, :, columns(cut)].astype(jnp.float32)
+
+        @pl.when(z < deep - 1)
+        def _():
+            part_in(deep, cut).wait_recv()
+            own[:, columns(cut)] += arrived[deep, :, columns(cut)].astype(jnp.float32)
+
+        mixed[:, columns(cut)] = own[:, columns(cut)].astype(jnp.bfloat16)
+
     def enter(i):
         unit_spread.hand_on((keep - 1) * deep + place(i))
         for e in range(keep):
             unit_spread.arrive(e * deep + place(i))
 
+    def give_back_all(zs, first, last):
+        for cut in range(first, last):
+            give_back(zs, cut)
+
+    def send_all(zs, first, last):
+        for cut in range(first, last):
+            send_part(zs, cut)
+
+    def come(i):
+        enter(i)
+        multiply(place(i), 0)
+        give_back_all(place(i), 0, per)
+
+    lead = deep - 2
+    inner = jnp.logical_not(end)
     enter(0)
     all_in([lower], 0)
     multiply(place(0), 0)
-
-    def turn_back(i):
-        enter(i + 1)
-        multiply(place(i + 1), 0)
-
-        @pl.when(i < deep - 2)
-        def _():
-            send_part(place(i), 0)
-
-    loop(0, deep - 1, turn_back)
-    for cut in range(1, HALVES):
-        all_in([lower], cut)
-        loop(0, deep, lambda i: multiply(place(i), cut))
-        send_part(place(deep - 2), cut - 1)
-        loop(0, deep - 2, lambda i: send_part(place(i), cut))
-    send_part(place(deep - 2), HALVES - 1)
-    for cut in range(HALVES):
-        add_up(z, cut)
-
-        @pl.when(z > 0)
-        def _():
-            part_in(z, cut).wait_recv()
-            total[...] += arrived[z, :, columns(cut)].astype(jnp.float32)
-
-        @pl.when(z < deep - 1)
-        def _():
-            part_in(deep, cut).wait_recv()
-            total[...] += arrived[deep, :, columns(cut)].astype(jnp.float32)
-
-        mixed[:, columns(cut)] = total[...].astype(jnp.bfloat16)
+    give_back_all(place(0), 0, per)
+
+    def second(i):
+        multiply(place(i), 1)
+        give_back_all(place(i), per, cuts)
+
+    def lead_in(i):
+        come(i)
+
+        @pl.when(inner & (i == 1))
+        def _():
+            all_in([lower], 1)
+            second(0)
+
+        send_all(place(i - 1), 0, per)
+
+    loop(1, lead, lead_in)
+    pl.when(inner)(lambda: loop(1, lead, second))
+    send_all(place(lead - 1), 0, per)
+    loop(lead, deep, come)
+
+    @pl.when(end)
+    def _():
+        all_in([lower], 1)
+        loop(0, lead, second)
+
+    pl.when(end)(lambda: send_part(place(lead), 0))
+    loop(lead, deep, second)
+
+    def lead_out(i):
+        send_all(place(i), per, cuts)
+
+        @pl.when(inner & (i == 0))
+        def _():
+            send_all(place(lead), 0, per)
+
+    loop(0, lead, lead_out)
+
+    @pl.when(end)
+    def _():
+        send_all(place(lead), 1, per)
+
+    send_all(place(lead), per, cuts)
+    for cut in range(cuts):
+        add_own(cut)
 
     def sent(turn):
         for part in [*pair, lower]:
@@ -619,10 +673,12 @@
 
     loop(0, n - 1, sent)
     loop(0, keep * deep, unit_spread.drain)
+    for cut in range(cuts):
+        finish(cut)
 
     def sent_back(i):
         zs = place(i)
-        for cut in range(HALVES):
+        for cut in range(cuts):
             others(lambda row: returning(zs, row, y, cut).wait_send())
 
             @pl.when(zs != z)
@@ -641,6 +697,7 @@
     _, unit_rows, width = down_master.shape
     tokens, model = prompt.shape
     keep = experts // n
+    cuts = 2 * HALVES if width % (2 * HALVES * 128) == 0 else HALVES
     capacity = 2 * tokens * routes.shape[1] // experts
     inside, anywhere = pl.BlockSpec(memory_space=pltpu.VMEM), pl.BlockSpec(memory_space=pl.ANY)
     half, full = jnp.bfloat16, jnp.float32
@@ -669,8 +726,9 @@
             pltpu.VMEM((keep, n * capacity, units * tp), half),
             pltpu.VMEM((deep, wide, keep, capacity, width), half),
             pltpu.VMEM((deep + 1, tokens, width), half),
-            pltpu.VMEM((wide * keep * capacity, tokens), half),
-            pltpu.VMEM((tokens, width // HALVES), full),
+            pltpu.VMEM((deep, wide * keep * capacity, tokens), half),
+            pltpu.VMEM((tokens, width // cuts), full),
+            pltpu.VMEM((tokens, width), full),
             pltpu.VMEM((rows, 1), full),
             dma((3, RING)),
             dma((3, n, HALVES)),
@@ -682,15 +740,15 @@
             dma((deep,)),
             dma((deep, wide)),
             dma((n,)),
-            dma((deep, wide, HALVES)),
-            dma((deep, wide, HALVES)),
-            dma((deep, HALVES)),
-            dma((deep + 1, HALVES)),
+            dma((deep, wide, cuts)),
+            dma((deep, wide, cuts)),
+            dma((deep, cuts)),
+            dma((deep + 1, cuts)),
             *[dma((n, chips))] * 4,
             *[dma((keep * deep, chips))] * 4,
         ],
         compiler_params=pltpu.CompilerParams(
-            collective_id=0, has_side_effects=True, vmem_limit_bytes=55 * 2**20
+            collective_id=0, has_side_effects=True, vmem_limit_bytes=56 * 2**20
         ),
         name="experts",
     )(norm_gain[None, :], routes.T, affinity.T, prompt, gate_master, up_master, down_master)

time: 230 us -> 226 us (0.983)
  Pallas kernels: 225 us -> 220 us
    pallas_call x1, Pallas kernels: 225 us -> 220 us  [per_device(): pl.pallas_call(functools.partial(kernel, n, tp, deep), out_shape=[pltpu.V...]
where the time goes in v4:
time: 226 us; the launch traced here: 225 us
  Pallas kernels  220 us (97%)
  local copies, waits for them, and re-layouts  4.48 us (2%)
    pallas_call x1, Pallas kernels, per_device(): pl.pallas_call(functools.partial(kernel, n, tp, deep), out_shape=[pltpu.V...  220 us

profile of v4, /device:TPU:0, one launch (start us, length us, event | category | flops | bytes accessed | tf_op | source)
XLA Modules:
  0.0 225.3 jit_solution(5850741912486281686)
XLA Ops:
  0.6 220.2 %experts.1 = (bf16[768,512]{1,0:T(8,128)(2,1)S(1)}, bf16[2,2048,512]{2,1,0:T(8,128)(2,1)S(1)}, bf16[2,1024,512]{2,1,0:T(8,128)(2,1)S(1)}) custom-call(f32[1,256]{1,0:T(1,128)} %bitcast.5, s32[2,768]{1,0:T(2,128)} %bitcast.3, f32[2,768]{1,0:T(2,128)} %bitcast.4, bf16[768,2048]{1,0:T(8,128)(2,1)} %prompt.1, f32[16,256,256]{2,1,0:T(8,128)} %gate.1, ...), custom_call_target="tpu_custom_call" | custom-call | tf_op jit(solution)/shard_map/experts/pallas_call | solution.py:705
  220.9 0.9 copy.13
  221.7 1.3 copy.14
  223.1 2.3 %fusion = (bf16[2,2048,256]{2,1,0:T(8,128)(2,1)}, bf16[2,2048,256]{2,1,0:T(8,128)(2,1)}) fusion(bf16[2,2048,512]{2,1,0:T(8,128)(2,1)S(1)} %get-tuple-element.8), kind=kLoop, calls=%fused_computation | loop fusion | bytes 8388608 | tf_op jit(solution)/shard_map/slice | solution.py:755
